TPU v7x, 32 devices: a whole 2x2x4 slice. The times are simulated.
32 devices in a mesh: ep: 8 (over z, x), tp: 4 (over y, core).
Axes of the slice: x: 2, y: 2, z: 4, core: 2. Of those that a mesh axis runs over, the one named last changes fastest.
Arguments:
- tokens: bfloat16 [256, 2048], P('ep'), may hold values from -6 to 6
- state: float32 [256, 16, 128, 128], P('ep', 'tp'), may hold values from -6 to 6
- norm_gain: float32 [2048], replicated, may hold values from 0.1 to 1.9
- w_query: bfloat16 [2048, 2048], P(None, 'tp'), may hold values from -0.125 to 0.125
- w_forget: bfloat16 [2048, 2048], P(None, 'tp'), may hold values from -0.125 to 0.125
- w_input: bfloat16 [2048, 2048], P(None, 'tp'), may hold values from -0.125 to 0.125
- w_outgate: bfloat16 [2048, 2048], P(None, 'tp'), may hold values from -0.125 to 0.125
- forget_floor: float32 [2048], P('tp'), may hold values from 0.05 to 0.95
- head_gain: float32 [128], replicated, may hold values from 0.1 to 1.9
- w_out: bfloat16 [2048, 2048], P('tp'), may hold values from -0.125 to 0.125
- ffn_gain: float32 [2048], replicated, may hold values from 0.1 to 1.9
- routes: int32 [256, 2], P('ep'), may hold values from 0 to 7, all different within a row; in each aligned block of 32 rows (0 to 31, 32 to 63, ...) at most 16 rows name the same one
- route_weights: float32 [256, 2], P('ep'), may hold values from 0.2 to 1
- expert_gate: bfloat16 [8, 2048, 5632], P('ep', None, 'tp'), may hold values from -0.125 to 0.125
- expert_up: bfloat16 [8, 2048, 5632], P('ep', None, 'tp'), may hold values from -0.125 to 0.125
- expert_down: bfloat16 [8, 5632, 2048], P('ep', 'tp'), may hold values from -0.078125 to 0.078125
- dense_gate: bfloat16 [2048, 5632], P(None, 'ep'), may hold values from -0.125 to 0.125
- dense_up: bfloat16 [2048, 5632], P(None, 'ep'), may hold values from -0.125 to 0.125
- dense_down: bfloat16 [5632, 2048], P('ep'), may hold values from -0.078125 to 0.078125
- dense_mix: float32 [2048], replicated, may hold values from -6 to 6
Outputs:
- mixed: bfloat16 [256, 2048], P('ep')
- new_state: float32 [256, 16, 128, 128], P('ep', 'tp')
Inputs may be any that keep to these rules, and one draw needn't show every extreme that they name: `routes`: each row names 2 different experts; the rows of one index of ep name no expert more than 16 times, a bound that some block reaches.
All inputs are finite; a program needn't handle non-finite values.
Results may differ from a plain program's by a relative error of at most 0.014.
Values may be sent and summed in bfloat16 or wider, within the bound.
A program may use at most 128 MiB of HBM per device.

v0:
```python
import jax
import jax.numpy as jnp
from jax import lax
from jax.sharding import PartitionSpec as P

EPS = 1e-06


def rms_norm(value, gain):
    return value * lax.rsqrt(jnp.mean(value * value, axis=-1, keepdims=True) + EPS) * gain


def make_table(local_routes, experts, capacity):
    flat = local_routes.reshape(-1)
    onehot = (flat[:, None] == jnp.arange(experts, dtype=jnp.int32)[None, :]).astype(jnp.int32)
    before = jnp.cumsum(onehot, axis=0) - onehot
    slot = jnp.sum(before * onehot, axis=1)
    where = flat * capacity + slot
    return (where[:, None] == jnp.arange(experts * capacity, dtype=jnp.int32)[None, :]).astype(
        jnp.bfloat16
    )


def local(
    tokens,
    state,
    norm_gain,
    w_query,
    w_forget,
    w_input,
    w_outgate,
    forget_floor,
    head_gain,
    w_out,
    ffn_gain,
    routes,
    route_weights,
    expert_gate,
    expert_up,
    expert_down,
    dense_gate,
    dense_up,
    dense_down,
    dense_mix,
):
    seqs, width = tokens.shape
    local_heads = state.shape[1]
    key_size = state.shape[2]
    value_size = state.shape[3]
    resid_in = tokens.astype(jnp.float32)
    normed = rms_norm(resid_in, norm_gain).astype(jnp.bfloat16)
    zq = jnp.dot(normed, w_query, preferred_element_type=jnp.float32)
    zf = jnp.dot(normed, w_forget, preferred_element_type=jnp.float32)
    zi = jnp.dot(normed, w_input, preferred_element_type=jnp.float32)
    zg = jnp.dot(normed, w_outgate, preferred_element_type=jnp.float32)
    logf = jnp.logaddexp(jax.nn.log_sigmoid(zf), jnp.log(forget_floor) + jax.nn.log_sigmoid(-zf))
    logf = logf.reshape(seqs, local_heads, key_size)
    query = jax.nn.silu(zq).reshape(seqs, local_heads, key_size)
    keep = jnp.exp(logf)
    write = -jnp.expm1(logf)
    values = zi.reshape(seqs, local_heads, value_size)
    new_state = keep[..., None] * state + write[..., None] * values[:, :, None, :]
    read = jnp.einsum("thk,thkv->thv", query, new_state, precision=lax.Precision.HIGHEST)
    read = rms_norm(read, head_gain).reshape(seqs, local_heads * value_size)
    headout = (read * jax.nn.silu(zg)).astype(jnp.bfloat16)
    block_term = jnp.dot(headout, w_out, preferred_element_type=jnp.float32)
    block_term = block_term.astype(jnp.bfloat16).astype(jnp.float32)
    mixout = lax.psum(block_term.astype(jnp.bfloat16), "tp").astype(jnp.float32)
    resid = resid_in + mixout
    ffn_in = rms_norm(resid, ffn_gain).astype(jnp.bfloat16)
    piece = lax.all_gather(ffn_in, "ep", axis=0, tiled=True)
    dgate = jnp.dot(piece, dense_gate, preferred_element_type=jnp.float32)
    dupper = jnp.dot(piece, dense_up, preferred_element_type=jnp.float32)
    dense_hidden = (jax.nn.silu(dgate) * dupper).astype(jnp.bfloat16)
    rows = dense_hidden
    summed = lax.psum_scatter(
        jnp.dot(rows, dense_down, preferred_element_type=jnp.float32).astype(jnp.bfloat16),
        "ep",
        scatter_dimension=0,
        tiled=True,
    )
    dense = summed.astype(jnp.float32)
    experts = lax.axis_size("ep") * expert_gate.shape[0]
    top = routes.shape[1]
    capacity = 2 * seqs * top // experts
    table = make_table(routes, experts, capacity)
    repeated = jnp.repeat(ffn_in, top, axis=0)
    sent = jnp.dot(table.T, repeated, preferred_element_type=jnp.float32).astype(jnp.bfloat16)
    sent = sent.reshape(experts, capacity, width)
    arrived = lax.all_to_all(sent, "ep", split_axis=0, concat_axis=0, tiled=True)
    sources, items, _ = arrived.shape
    rows = arrived.reshape(sources * items, width)
    gate = jnp.dot(rows, expert_gate[0], preferred_element_type=jnp.float32)
    upper = jnp.dot(rows, expert_up[0], preferred_element_type=jnp.float32)
    hidden = (jax.nn.silu(gate) * upper).astype(jnp.bfloat16)
    part = jnp.dot(hidden, expert_down[0], preferred_element_type=jnp.float32)
    part = part.astype(jnp.bfloat16).astype(jnp.float32)
    summed_parts = lax.psum(part.astype(jnp.bfloat16), "tp")
    results = summed_parts.reshape(sources, items, width)
    back = lax.all_to_all(results, "ep", split_axis=0, concat_axis=0, tiled=True)
    picked = jnp.dot(
        table, back.reshape(experts * capacity, width), preferred_element_type=jnp.float32
    )
    weighted = picked * route_weights.reshape(seqs * top)[:, None]
    moe = jnp.sum(weighted.reshape(seqs, top, width), axis=1)
    mixed = (resid + moe + jax.nn.sigmoid(dense_mix) * dense).astype(jnp.bfloat16)
    return (mixed, new_state)


def solution(mesh):
    in_specs = (
        P("ep", None),
        P("ep", "tp", None, None),
        P(),
        P(None, "tp"),
        P(None, "tp"),
        P(None, "tp"),
        P(None, "tp"),
        P("tp"),
        P(),
        P("tp", None),
        P(),
        P("ep", None),
        P("ep", None),
        P("ep", None, "tp"),
        P("ep", None, "tp"),
        P("ep", "tp", None),
        P(None, "ep"),
        P(None, "ep"),
        P("ep", None),
        P(),
    )
    out_specs = (P("ep", None), P("ep", "tp", None, None))
    return jax.shard_map(local, mesh=mesh, in_specs=in_specs, out_specs=out_specs, check_vma=False)
```

profile of v0, /device:TPU:0, one launch (start us, length us, event | category | flops | bytes accessed | tf_op | source)
XLA Modules:
  0.0 235.8 jit_solution(614285579938243527)
XLA Ops:
  7.2 0.0 copy-start
  7.2 0.0 all-reduce.3.cloned.1.call-start
  7.3 1.2 fusion.20
  8.5 2.2 divide_multiply_fusion
  10.7 2.2 fusion.38
  13.0 2.3 fusion.35
  15.3 8.2 %multiply_add_fusion = f32[32,4,128,128]{3,2,1,0:T(8,128)S(1)} fusion(f32[32,4,128,128]{3,2,1,0:T(8,128)} %param.21, f32[32,4,128]{2,1,0:T(4,128)S(1)} %mul.144, f32[32,4,128]{2,1,0:T(4,128)S(1)} %neg.60, f32[32,4,128]{2,1,0:T(4,128)S(1)} %exp.44), kind=kLoop, calls=%fused_computation | loop fusion | flops 6291456 | bytes 16973824 | tf_op jit(solution)/shard_map/add | solution.py:62
  23.5 0.0 copy-start.1
  23.6 7.3 %fusion.50 = f32[32,4,1,128]{3,2,1,0:T(1,128)S(1)} fusion(f32[32,4,128,1]{2,3,1,0:T(1,128)S(1)} %bitcast.52, f32[32,4,128,128]{3,2,1,0:T(8,128)S(1)} %multiply_add_fusion), kind=kOutput, calls=%fused_computation.59 | convolution fusion | flops 25165824 | bytes 8519680 | tf_op jit(solution)/shard_map/thk,thkv->thv/dot_general | solution.py:63
  30.8 0.1 multiply_reduce_fusion.1
  31.0 0.1 multiply_multiply_fusion
  31.1 3.8 %convolution_convert_fusion.2 = bf16[32,2048]{1,0:T(8,128)(2,1)} fusion(bf16[512,2048]{1,0:T(8,128)(2,1)} %param.29, f32[4,8,4,128]{3,2,1,0:T(4,128)S(1)} %bitcast.53, bf16[2048,512]{1,0:T(8,128)(2,1)} %param.26, bf16[32,2048]{1,0:T(8,128)(2,1)S(1)} %copy-done.2, f32[2048]{0:T(1024)S(1)} %copy-done.4, f32[32]{0:T(128)S(1)} %add_rsqrt_fusion.2), kind=kOutput, calls=%fused_computation.13 | convolution fusion | flops 134643712 | bytes 4530304 | tf_op jit(solution)/shard_map/dot_general | solution.py:66
  34.9 0.0 all-reduce.3.cloned.1.call-update
  35.0 0.1 copy.24
  35.0 0.1 reshape.88
  35.1 0.1 fusion.28
  35.2 0.1 reduce_window_sum.11
  35.3 0.2 select_reduce_fusion
  35.5 34.1 %all-reduce.3.cloned.1.call-done = bf16[32,2048]{1,0:T(8,128)(2,1)} async-done(((bf16[32,2048]{1,0:T(8,128)(2,1)}), bf16[32,2048]{1,0:T(8,128)(2,1)}) %all-reduce.3.cloned.1.call-update) | async-done | bytes 131088 | tf_op jit(solution)/shard_map/psum | solution.py:68
  69.6 1.1 multiply_reduce_fusion
  70.7 1.0 multiply_convert_fusion
  71.7 0.1 broadcast_in_dim.2
  71.9 0.8 reshape.89
  72.6 2.1 convolution_convert_fusion.1
  74.8 5.5 %all-to-all-start = ((bf16[8,16,2048]{2,1,0:T(8,128)(2,1)}), bf16[8,16,2048]{2,1,0:T(8,128)(2,1)S(1)}, u32[]{:S(2)}, u32[]{:S(2)}) async-start(bf16[8,16,2048]{2,1,0:T(8,128)(2,1)} %bitcast.3), calls=%async_computation | async-start | bytes 1048576 | tf_op jit(solution)/shard_map/all_to_all | solution.py:90
  80.3 0.0 all-gather.2.cloned.1.call-start
  80.4 0.7 all-gather.2.cloned.1.call-update
  81.1 0.2 all-reduce.5.cloned.1.call-start
  81.3 12.4 %all-to-all-done = bf16[8,16,2048]{2,1,0:T(8,128)(2,1)S(1)} async-done(((bf16[8,16,2048]{2,1,0:T(8,128)(2,1)}), bf16[8,16,2048]{2,1,0:T(8,128)(2,1)S(1)}, u32[]{:S(2)}, u32[]{:S(2)}) %all-to-all-start) | async-done | bytes 524320 | tf_op jit(solution)/shard_map/all_to_all | solution.py:90
  93.7 4.5 %fusion.4 = f32[128,1408]{1,0:T(8,128)} fusion(bf16[128,2048]{1,0:T(8,128)(2,1)S(1)} %bitcast.47, bf16[1,2048,1408]{2,1,0:T(8,128)(2,1)} %param.33), kind=kOutput, calls=%fused_computation.5 | convolution fusion | flops 738197504 | bytes 7012352 | tf_op jit(solution)/shard_map/dot_general | solution.py:93
  98.2 7.3 %fusion.12 = bf16[128,2048]{1,0:T(8,128)(2,1)} fusion(bf16[1,1408,2048]{2,1,0:T(8,128)(2,1)} %param.35, bf16[128,2048]{1,0:T(8,128)(2,1)S(1)} %bitcast.48, bf16[1,2048,1408]{2,1,0:T(8,128)(2,1)} %param.34, f32[128,1408]{1,0:T(8,128)} %fusion.4), kind=kOutput, calls=%fused_computation.11 | convolution fusion | flops 1477738496 | bytes 13303808 | tf_op jit(solution)/shard_map/dot_general | solution.py:96
  105.5 0.0 all-reduce.5.cloned.1.call-update
  105.5 0.0 reduce-scatter.2.cloned.1.call-start
  105.6 19.0 %all-gather.2.cloned.1.call-done = bf16[256,2048]{1,0:T(8,128)(2,1)} async-done(((bf16[32,2048]{1,0:T(8,128)(2,1)}), bf16[256,2048]{1,0:T(8,128)(2,1)}) %all-gather.2.cloned.1.call-update) | async-done | bytes 1048592 | tf_op jit(solution)/shard_map/all_gather | solution.py:71
  124.6 4.0 %fusion.51 = f32[256,704]{0,1:T(8,128)} fusion(bf16[256,2048]{1,0:T(8,128)(2,1)} %all-gather.2.cloned.1.call-done, bf16[2048,704]{0,1:T(8,128)(2,1)} %param.36), kind=kOutput, calls=%fused_computation.60 | convolution fusion | flops 738197504 | bytes 4653056 | tf_op jit(solution)/shard_map/dot_general | solution.py:72
  128.6 6.6 %convolution_convert_fusion = bf16[256,2048]{1,0:T(8,128)(2,1)} fusion(bf16[704,2048]{1,0:T(8,128)(2,1)S(1)} %copy-done, bf16[256,2048]{1,0:T(8,128)(2,1)} %all-gather.2.cloned.1.call-done, bf16[2048,704]{0,1:T(8,128)(2,1)} %param.37, f32[256,704]{0,1:T(8,128)} %fusion.51), kind=kOutput, calls=%fused_computation.7 | convolution fusion | flops 1478000640 | bytes 8585216 | tf_op jit(solution)/shard_map/dot_general | solution.py:77
  135.2 0.0 reduce-scatter.2.cloned.1.call-update
  135.2 23.9 %all-reduce.5.cloned.1.call-done = bf16[8,16,2048]{2,1,0:T(8,128)(2,1)} async-done(((bf16[8,16,2048]{2,1,0:T(8,128)(2,1)}), bf16[8,16,2048]{2,1,0:T(8,128)(2,1)}) %all-reduce.5.cloned.1.call-update) | async-done | bytes 524304 | tf_op jit(solution)/shard_map/psum | solution.py:98
  159.1 5.5 %all-to-all-start.1 = ((bf16[8,16,2048]{2,1,0:T(8,128)(2,1)}), bf16[8,16,2048]{2,1,0:T(8,128)(2,1)S(1)}, u32[]{:S(2)}, u32[]{:S(2)}) async-start(bf16[8,16,2048]{2,1,0:T(8,128)(2,1)} %all-reduce.5.cloned.1.call-done), calls=%async_computation.1 | async-start | bytes 1048576 | tf_op jit(solution)/shard_map/all_to_all | solution.py:100
  164.6 0.8 copy.25
  165.4 0.6 mul.164
  166.0 0.7 add_divide_fusion
  166.7 15.4 %all-to-all-done.1 = bf16[8,16,2048]{2,1,0:T(8,128)(2,1)S(1)} async-done(((bf16[8,16,2048]{2,1,0:T(8,128)(2,1)}), bf16[8,16,2048]{2,1,0:T(8,128)(2,1)S(1)}, u32[]{:S(2)}, u32[]{:S(2)}) %all-to-all-start.1) | async-done | bytes 524320 | tf_op jit(solution)/shard_map/all_to_all | solution.py:100
  182.1 1.8 convolution_multiply_fusion
  183.8 1.4 reshape.94
  185.2 1.3 reduce_sum.49
  186.5 40.9 %reduce-scatter.2.cloned.1.call-done = bf16[32,2048]{1,0:T(8,128)(2,1)} async-done(((bf16[256,2048]{1,0:T(8,128)(2,1)}), bf16[32,2048]{1,0:T(8,128)(2,1)}) %reduce-scatter.2.cloned.1.call-update) | async-done | bytes 131088 | tf_op jit(solution)/shard_map/reduce_scatter | solution.py:76
  227.5 1.8 add_convert_fusion
  (27 shorter events, 0.2 us)
Async XLA Ops:
  7.2 121.4 %copy-start = (bf16[704,2048]{1,0:T(8,128)(2,1)S(1)}, bf16[704,2048]{1,0:T(8,128)(2,1)}, u32[]{:S(2)}) copy-start(bf16[704,2048]{1,0:T(8,128)(2,1)} %param.38) | copy-start | bytes 8650756
  7.2 5.8 %copy-start.2 = (bf16[32,2048]{1,0:T(8,128)(2,1)S(1)}, bf16[32,2048]{1,0:T(8,128)(2,1)}, u32[]{:S(2)}) copy-start(bf16[32,2048]{1,0:T(8,128)(2,1)} %param.20) | copy-start | bytes 393220
  7.2 5.8 %copy-start.4 = (f32[2048]{0:T(1024)S(1)}, f32[2048]{0:T(1024)}, u32[]{:S(2)}) copy-start(f32[2048]{0:T(1024)} %param.22) | copy-start | bytes 24580
  7.2 5.7 %copy-start.7 = (f32[512]{0:T(512)S(1)}, f32[512]{0:T(512)}, u32[]{:S(2)}) copy-start(f32[512]{0:T(512)} %param.27) | copy-start | bytes 6148
  7.2 62.4 %all-reduce.3.cloned.1.call-start = ((), (), s32[]{:S(2)}) async-start(), calls=%async_computation.3 | async-start | bytes 262144 | tf_op jit(solution)/shard_map/psum | solution.py:68
  23.5 7.3 %copy-start.1 = (f32[32,4,128,128]{3,2,1,0:T(8,128)}, f32[32,4,128,128]{3,2,1,0:T(8,128)S(1)}, u32[]{:S(2)}) copy-start(f32[32,4,128,128]{3,2,1,0:T(8,128)S(1)} %multiply_add_fusion) | copy-start | bytes 25165828
  23.6 7.4 %copy-start.9 = (f32[128]{0:T(128)S(1)}, f32[128]{0:T(128)}, u32[]{:S(2)}) copy-start(f32[128]{0:T(128)} %param.28) | copy-start | bytes 1540
  30.8 4.1 %copy-start.8 = (s32[32,2]{0,1:T(2,128)S(1)}, s32[32,2]{0,1:T(2,128)}, u32[]{:S(2)}) copy-start(s32[32,2]{0,1:T(2,128)} %param.31) | copy-start | bytes 772
  30.8 39.9 %copy-start.5 = (f32[2048]{0:T(1024)S(1)}, f32[2048]{0:T(1024)}, u32[]{:S(2)}) copy-start(f32[2048]{0:T(1024)} %param.30) | copy-start | bytes 24580
  35.5 39.3 %copy-start.6 = (s32[64]{0:T(128)}, s32[64]{0:T(128)S(1)}, u32[]{:S(2)}) copy-start(s32[64]{0:T(128)S(1)} %multiply_add_fusion.1) | copy-start | bytes 772
  71.7 3.1 %copy-start.3 = (bf16[32,2048]{1,0:T(8,128)(2,1)}, bf16[32,2048]{1,0:T(8,128)(2,1)S(1)}, u32[]{:S(2)}) copy-start(bf16[32,2048]{1,0:T(8,128)(2,1)S(1)} %multiply_convert_fusion) | copy-start | bytes 393220
  74.8 18.9 %all-to-all-start = ((bf16[8,16,2048]{2,1,0:T(8,128)(2,1)}), bf16[8,16,2048]{2,1,0:T(8,128)(2,1)S(1)}, u32[]{:S(2)}, u32[]{:S(2)}) async-start(bf16[8,16,2048]{2,1,0:T(8,128)(2,1)} %bitcast.3), calls=%async_computation | async-start | bytes 1048576 | tf_op jit(solution)/shard_map/all_to_all | solution.py:90
  80.3 44.3 %all-gather.2.cloned.1.call-start = ((), (), s32[]{:S(2)}) async-start(), calls=%async_computation.5 | async-start | bytes 1179648 | tf_op jit(solution)/shard_map/all_gather | solution.py:71
  81.1 78.1 %all-reduce.5.cloned.1.call-start = ((), (), s32[]{:S(2)}) async-start(), calls=%async_computation.4 | async-start | bytes 1048576 | tf_op jit(solution)/shard_map/psum | solution.py:98
  105.5 121.9 %reduce-scatter.2.cloned.1.call-start = ((), (), s32[]{:S(2)}) async-start(), calls=%async_computation.6 | async-start | bytes 1179648 | tf_op jit(solution)/shard_map/reduce_scatter | solution.py:76
  159.1 23.0 %all-to-all-start.1 = ((bf16[8,16,2048]{2,1,0:T(8,128)(2,1)}), bf16[8,16,2048]{2,1,0:T(8,128)(2,1)S(1)}, u32[]{:S(2)}, u32[]{:S(2)}) async-start(bf16[8,16,2048]{2,1,0:T(8,128)(2,1)} %all-reduce.5.cloned.1.call-done), calls=%async_computation.1 | async-start | bytes 1048576 | tf_op jit(solution)/shard_map/all_to_all | solution.py:100
Sparse Core Ops, SparseCore 0:
  35.1 34.4 all-reduce.2
  83.8 40.7 all-gather.1
  127.0 32.1 all-reduce.4
  162.4 65.0 reduce-scatter.1
where the time goes:
time: 237 us; the launch traced here: 236 us
  waiting for transfers between devices  147 us (62%)
  matrix products  44 us (19%)
  other arithmetic  15.9 us (7%)
  between operations  14 us (6%)
  starting transfers between devices  11.4 us (5%)
  local copies, waits for them, and re-layouts  4.03 us (2%)
    reduce_scatter x1, waiting for transfers between devices, local(): lax.psum_scatter(jnp.dot(rows, dense_down, preferred_element_type=jnp.flo...  40.9 us
    psum x1, waiting for transfers between devices, local(): mixout = lax.psum(block_term.astype(jnp.bfloat16), 'tp').astype(jnp.float32)  34.1 us
    psum x1, waiting for transfers between devices, local(): summed_parts = lax.psum(part.astype(jnp.bfloat16), 'tp')  23.9 us
    all_gather x1, waiting for transfers between devices, local(): piece = lax.all_gather(ffn_in, 'ep', axis=0, tiled=True)  19 us
    all_to_all x1, waiting for transfers between devices, local(): lax.all_to_all(results, 'ep', split_axis=0, concat_axis=0, tiled=True)  15.4 us
    all_to_all x1, waiting for transfers between devices, local(): lax.all_to_all(sent, 'ep', split_axis=0, concat_axis=0, tiled=True)  12.4 us
    add x1, other arithmetic, local(): keep[..., None] * state + write[..., None] * values[:, :, None, :]  8.22 us
    dot_general x1, matrix products, local(): part = jnp.dot(hidden, expert_down[0], preferred_element_type=jnp.float32)  7.29 us
  transfers between devices with their start and end apart: 6, of which 6 were waited for; matrix products, arithmetic and copies ran while one was open for 12% of the time, Pallas kernels for 0%

commit v1 on v0

--- a/solution.py
+++ b/solution.py
@@ -1,6 +1,10 @@
+import functools
+
 import jax
 import jax.numpy as jnp
 from jax import lax
+from jax.experimental import pallas as pl
+from jax.experimental.pallas import tpu as pltpu
 from jax.sharding import PartitionSpec as P
 
 EPS = 1e-06
@@ -19,6 +23,372 @@
     return (where[:, None] == jnp.arange(experts * capacity, dtype=jnp.int32)[None, :]).astype(
         jnp.bfloat16
     )
+
+
+def channel_kernel(
+    ep_size,
+    tp_size,
+    tok_ref,
+    bt_ref,
+    gain_ref,
+    mix_ref,
+    routes_ref,
+    rw_ref,
+    eg_hbm,
+    eu_hbm,
+    ed_hbm,
+    dg_hbm,
+    du_hbm,
+    dd_hbm,
+    out_ref,
+    eg,
+    eu,
+    ed,
+    dg,
+    du,
+    dd,
+    rs_buf,
+    xg,
+    wt,
+    wg,
+    wcol,
+    x2d,
+    hid,
+    dhid,
+    resid_ref,
+    cbuf,
+    crecv,
+    ysend,
+    yrecv,
+    esend,
+    erecv,
+    fbuf,
+    ld_sem,
+    rs_s,
+    rs_r,
+    w_s,
+    w_r,
+    ag_s,
+    g_r,
+    gy_s,
+    gc_s,
+    cr_s,
+    cr_r,
+    yr_s,
+    yr_r,
+    er_s,
+    er_r,
+    f_s,
+    f_r,
+):
+    E, T = ep_size, tp_size
+    Y = T // 2
+    e, t = lax.axis_index("ep"), lax.axis_index("tp")
+    y, c = t // 2, t % 2
+    partner = y * 2 + (1 - c)
+    rows, width = resid_ref.shape
+    seqs = T * rows
+    units = dg.shape[0]
+    hidden_units = eg.shape[1]
+
+    def rcopy(src, dst, ssem, rsem, ee, tt):
+        return pltpu.make_async_remote_copy(
+            src_ref=src,
+            dst_ref=dst,
+            send_sem=ssem,
+            recv_sem=rsem,
+            device_id={"ep": ee, "tp": tt},
+            device_id_type=pl.DeviceIdType.MESH,
+        )
+
+    mine = pl.ds(pl.multiple_of(t * units, 16), units)
+    loads = [
+        pltpu.make_async_copy(dg_hbm.at[mine], dg, ld_sem.at[0]),
+        pltpu.make_async_copy(du_hbm.at[mine], du, ld_sem.at[1]),
+        pltpu.make_async_copy(eg_hbm, eg, ld_sem.at[2]),
+        pltpu.make_async_copy(eu_hbm, eu, ld_sem.at[3]),
+        pltpu.make_async_copy(ed_hbm, ed, ld_sem.at[4]),
+        pltpu.make_async_copy(dd_hbm.at[mine], dd, ld_sem.at[5]),
+    ]
+    barrier = pltpu.get_barrier_semaphore()
+    for i in range(1, E):
+        pl.semaphore_signal(
+            barrier, inc=1, device_id={"ep": (e + i) % E, "tp": t}, device_id_type=pl.DeviceIdType.MESH
+        )
+    for i in range(1, T):
+        pl.semaphore_signal(
+            barrier, inc=1, device_id={"ep": e, "tp": (t + i) % T}, device_id_type=pl.DeviceIdType.MESH
+        )
+    for cp in loads:
+        cp.start()
+
+    which = lax.broadcasted_iota(jnp.int32, (E, seqs), 0)
+    table = jnp.zeros((E, seqs), jnp.float32)
+    for k in range(routes_ref.shape[0]):
+        table = table + jnp.where(routes_ref[k : k + 1, :] == which, rw_ref[k : k + 1, :], 0.0)
+    wt[...] = jnp.zeros(wt.shape, jnp.float32)
+    wt[:, :seqs] = table
+
+    pl.semaphore_wait(barrier, E + T - 2)
+
+    sends = []
+    for i in range(1, T):
+        j = (t + i) % T
+        cp = rcopy(bt_ref.at[j], rs_buf.at[t], rs_s.at[j], rs_r.at[t], e, j)
+        cp.start()
+        sends.append(cp)
+    far = [E // 2]
+    for i in range(1, E // 2):
+        far = [i, E - i] + far
+    near, far = far, far[::-1]
+    for i in far:
+        j = (e + i) % E
+        cp = rcopy(wt, wg.at[e], w_s.at[j], w_r.at[e], j, t)
+        cp.start()
+        sends.append(cp)
+
+    resid = tok_ref[t].astype(jnp.float32) + bt_ref[t].astype(jnp.float32)
+    for i in range(1, T):
+        j = (t + i) % T
+        rcopy(rs_buf.at[j], rs_buf.at[j], rs_s.at[j], rs_r.at[j], e, j).wait_recv()
+        resid = resid + rs_buf[j].astype(jnp.float32)
+    resid_ref[...] = resid
+    normed = rms_norm(resid, gain_ref[...])
+    xg[e, t] = normed.astype(jnp.bfloat16)
+
+    for i in far:
+        j = (e + i) % E
+        cp = rcopy(xg.at[e, t], xg.at[e, t], ag_s.at[j], g_r.at[e, t], j, t)
+        cp.start()
+        sends.append(cp)
+
+    def forward(source):
+        for k in range(1, Y):
+            yy = (y + k) % Y
+            cp = rcopy(
+                xg.at[source, t], xg.at[source, t], gy_s.at[source, yy], g_r.at[source, t], e, yy * 2 + c
+            )
+            cp.start()
+            sends.append(cp)
+        forward_core(source, y)
+
+    def forward_core(source, yy):
+        col = yy * 2 + c
+        cp = rcopy(
+            xg.at[source, col], xg.at[source, col], gc_s.at[source, yy], g_r.at[source, col], e, partner
+        )
+        cp.start()
+        sends.append(cp)
+
+    def arrived(source, col):
+        rcopy(
+            xg.at[source, col], xg.at[source, col], ag_s.at[source], g_r.at[source, col], source, col
+        ).wait_recv()
+
+    forward(e)
+    order = [0] + near
+    diag = lax.broadcasted_iota(jnp.int32, (seqs, wt.shape[1]), 0) == lax.broadcasted_iota(
+        jnp.int32, (seqs, wt.shape[1]), 1
+    )
+    for i in near:
+        source = (e + i) % E
+        arrived(source, t)
+        forward(source)
+    for i in order:
+        source = (e + i) % E
+        for k in range(1, Y):
+            yy = (y + k) % Y
+            arrived(source, yy * 2 + c)
+            forward_core(source, yy)
+        if i == 0:
+            line = wt[pl.ds(e, 1), :]
+        else:
+            rcopy(wg.at[source], wg.at[source], w_s.at[source], w_r.at[source], source, t).wait_recv()
+            line = wg[source, pl.ds(e, 1), :]
+        column = jnp.sum(jnp.where(diag, line, 0.0), axis=1, keepdims=True)
+        at = pl.ds(pl.multiple_of(source * seqs, seqs), seqs)
+        wcol[at, :] = jnp.broadcast_to(column, (seqs, wcol.shape[1]))
+    for i in order:
+        source = (e + i) % E
+        for yy in range(Y):
+            arrived(source, yy * 2 + (1 - c))
+        at = pl.ds(pl.multiple_of(source * seqs, seqs), seqs)
+        x2d[at, :] = xg[source].astype(jnp.float32).reshape(seqs, width).astype(jnp.bfloat16)
+
+    across = (((1,), (1,)), ((), ()))
+    loads[0].wait()
+    loads[1].wait()
+    dgate = lax.dot_general(x2d[...], dg[...], across, preferred_element_type=jnp.float32)
+    dupper = lax.dot_general(x2d[...], du[...], across, preferred_element_type=jnp.float32)
+    dhid[...] = (jax.nn.silu(dgate) * dupper).astype(jnp.bfloat16)
+    loads[2].wait()
+    loads[3].wait()
+
+    def hidden_at(cols):
+        gate = jnp.dot(x2d[...], eg[:, cols], preferred_element_type=jnp.float32)
+        upper = jnp.dot(x2d[...], eu[:, cols], preferred_element_type=jnp.float32)
+        hid[:, cols] = (jax.nn.silu(gate) * upper).astype(jnp.bfloat16)
+
+    step = 256
+    whole_steps = hidden_units // step
+
+    @pl.loop(0, whole_steps)
+    def _(n):
+        hidden_at(pl.ds(pl.multiple_of(n * step, step), step))
+
+    if hidden_units % step:
+        hidden_at(pl.ds(whole_steps * step, hidden_units % step))
+    loads[4].wait()
+    loads[5].wait()
+
+    @pl.loop(0, width // step)
+    def _(n):
+        cols = pl.ds(pl.multiple_of(n * step, step), step)
+        expert = jnp.dot(hid[...], ed[:, cols], preferred_element_type=jnp.float32)
+        dense = jnp.dot(dhid[...], dd[:, cols], preferred_element_type=jnp.float32)
+        both = wcol[:, :1] * expert + jax.nn.sigmoid(mix_ref[:, cols]) * dense
+        both = both.reshape(E, T, rows, step).astype(jnp.bfloat16)
+        for j in range(T):
+            cbuf[j % 2, j // 2, :, :, cols] = both[:, j]
+
+    others = []
+    for k in range(Y):
+        yy = (y + 1 + k) % Y
+        cp = rcopy(cbuf.at[1 - c, yy], crecv.at[yy], cr_s.at[yy], cr_r.at[yy], e, partner)
+        cp.start()
+        sends.append(cp)
+        others.append(yy)
+
+    def core_sum(yy, block):
+        return cbuf[c, yy, block].astype(jnp.float32) + crecv[yy, block].astype(jnp.float32)
+
+    def core_arrived(yy):
+        rcopy(crecv.at[yy], crecv.at[yy], cr_s.at[yy], cr_r.at[yy], e, partner).wait_recv()
+
+    for yy in others[:-1]:
+        core_arrived(yy)
+        for i in far + [0]:
+            block = (e + i) % E
+            ysend[yy, block] = core_sum(yy, block).astype(jnp.bfloat16)
+            cp = rcopy(
+                ysend.at[yy, block], yrecv.at[y, block], yr_s.at[yy, block], yr_r.at[y, block], e, yy * 2 + c
+            )
+            cp.start()
+            sends.append(cp)
+    core_arrived(y)
+    total = None
+    for i in far + [0]:
+        block = (e + i) % E
+        total = core_sum(y, block)
+        for yy in others[:-1]:
+            rcopy(
+                yrecv.at[yy, block], yrecv.at[yy, block], yr_s.at[yy, block], yr_r.at[yy, block], e, yy * 2 + c
+            ).wait_recv()
+            total = total + yrecv[yy, block].astype(jnp.float32)
+        if i:
+            esend[block] = total.astype(jnp.bfloat16)
+            cp = rcopy(esend.at[block], erecv.at[e], er_s.at[block], er_r.at[e], block, t)
+            cp.start()
+            sends.append(cp)
+    total = total + resid_ref[...]
+    for i in near:
+        source = (e + i) % E
+        rcopy(erecv.at[source], erecv.at[source], er_s.at[source], er_r.at[source], source, t).wait_recv()
+        total = total + erecv[source].astype(jnp.float32)
+    fbuf[t] = total.astype(jnp.bfloat16)
+    for i in range(1, T):
+        j = (t + i) % T
+        cp = rcopy(fbuf.at[t], fbuf.at[t], f_s.at[j], f_r.at[t], e, j)
+        cp.start()
+        sends.append(cp)
+    for i in range(1, T):
+        j = (t + i) % T
+        rcopy(fbuf.at[j], fbuf.at[j], f_s.at[j], f_r.at[j], e, j).wait_recv()
+    out_ref[...] = fbuf[...]
+    for cp in sends:
+        cp.wait_send()
+
+
+def channel_mixers(tokens, term, ffn_gain, dense_mix, routes, route_weights, expert, dense):
+    E, T = lax.axis_size("ep"), lax.axis_size("tp")
+    Y = T // 2
+    seqs, width = tokens.shape
+    rows = seqs // T
+    eg, eu, ed = expert
+    dg, du, dd = dense
+    units = dg.shape[0] // T
+    hidden_units = eg.shape[1]
+    bf, f32 = jnp.bfloat16, jnp.float32
+    vmem, dma = pltpu.VMEM, pltpu.SemaphoreType.DMA
+    block = (rows, width)
+    total = E * seqs
+    vm = pl.BlockSpec(memory_space=pltpu.VMEM)
+    hbm = pl.BlockSpec(memory_space=pl.ANY)
+    out = pl.pallas_call(
+        functools.partial(channel_kernel, E, T),
+        out_shape=jax.ShapeDtypeStruct((T,) + block, bf),
+        in_specs=[vm] * 6 + [hbm] * 6,
+        out_specs=vm,
+        scratch_shapes=[
+            vmem(eg.shape, bf),
+            vmem(eu.shape, bf),
+            vmem(ed.shape, bf),
+            vmem((units, width), bf),
+            vmem((units, width), bf),
+            vmem((units, width), bf),
+            vmem((T,) + block, bf),
+            vmem((E, T) + block, bf),
+            vmem((E, 128), f32),
+            vmem((E, E, 128), f32),
+            vmem((total, 128), f32),
+            vmem((total, width), bf),
+            vmem((total, hidden_units), bf),
+            vmem((total, units), bf),
+            vmem(block, f32),
+            vmem((2, Y, E) + block, bf),
+            vmem((Y, E) + block, bf),
+            vmem((Y, E) + block, bf),
+            vmem((Y, E) + block, bf),
+            vmem((E,) + block, bf),
+            vmem((E,) + block, bf),
+            vmem((T,) + block, bf),
+            dma((6,)),
+            dma((T,)),
+            dma((T,)),
+            dma((E,)),
+            dma((E,)),
+            dma((E,)),
+            dma((E, T)),
+            dma((E, Y)),
+            dma((E, Y)),
+            dma((Y,)),
+            dma((Y,)),
+            dma((Y, E)),
+            dma((Y, E)),
+            dma((E,)),
+            dma((E,)),
+            dma((T,)),
+            dma((T,)),
+        ],
+        compiler_params=pltpu.CompilerParams(
+            collective_id=0, has_side_effects=True, vmem_limit_bytes=50 * 1024 * 1024
+        ),
+        name="channel_mixers",
+    )(
+        tokens.reshape((T,) + block),
+        term.reshape((T,) + block),
+        ffn_gain.reshape(1, width),
+        dense_mix.reshape(1, width),
+        routes.T,
+        route_weights.T,
+        eg,
+        eu,
+        ed,
+        dg,
+        du,
+        dd,
+    )
+    return out.reshape(seqs, width)
 
 
 def local(
@@ -64,6 +434,19 @@
     read = rms_norm(read, head_gain).reshape(seqs, local_heads * value_size)
     headout = (read * jax.nn.silu(zg)).astype(jnp.bfloat16)
     block_term = jnp.dot(headout, w_out, preferred_element_type=jnp.float32)
+    ways = lax.axis_size("tp")
+    if ways % 2 == 0 and seqs % (8 * ways) == 0 and dense_gate.shape[1] % (16 * ways) == 0:
+        mixed = channel_mixers(
+            tokens,
+            block_term.astype(jnp.bfloat16),
+            ffn_gain,
+            dense_mix,
+            routes,
+            route_weights,
+            (expert_gate[0], expert_up[0], expert_down[0]),
+            (dense_gate.T, dense_up.T, dense_down),
+        )
+        return (mixed, new_state)
     block_term = block_term.astype(jnp.bfloat16).astype(jnp.float32)
     mixout = lax.psum(block_term.astype(jnp.bfloat16), "tp").astype(jnp.float32)
     resid = resid_in + mixout

time: 237 us -> 82.7 us (0.35)
  waiting for transfers between devices: 147 us -> 0 us
  Pallas kernels: 0 us -> 49.1 us
  matrix products: 44 us -> 16.9 us
  between operations: 14 us -> 0.85 us
  starting transfers between devices: 11.4 us -> 0 us
  other arithmetic: 15.9 us -> 12.1 us
    psum x2 -> x0, waiting for transfers between devices: 58 us -> none  [the longest x1 34.1 us: local(): mixout = lax.psum(block_term.astype(jnp.bfloat16), 'tp').astype(jnp.float32)]
    pallas_call x0 -> x1, Pallas kernels: none -> 49.1 us  [channel_mixers(): pl.pallas_call(functools.partial(channel_kernel, E, T), out_shape=jax.Sha...]
    reduce_scatter x1 -> x0, waiting for transfers between devices: 40.9 us -> none  [local(): lax.psum_scatter(jnp.dot(rows, dense_down, preferred_element_type=jnp.flo...]
    all_to_all x2 -> x0, waiting for transfers between devices: 27.8 us -> none  [the longest x1 15.4 us: local(): lax.all_to_all(results, 'ep', split_axis=0, concat_axis=0, tiled=True)]
    dot_general x6 -> x0, matrix products: 26.2 us -> none  [the longest x1 7.29 us: local(): part = jnp.dot(hidden, expert_down[0], preferred_element_type=jnp.float32)]
    all_gather x1 -> x0, waiting for transfers between devices: 19 us -> none  [local(): piece = lax.all_gather(ffn_in, 'ep', axis=0, tiled=True)]
    all_to_all x2 -> x0, starting transfers between devices: 11 us -> none  [the longest x1 5.51 us: local(): lax.all_to_all(results, 'ep', split_axis=0, concat_axis=0, tiled=True)]
    convert_element_type x3 -> x0, other arithmetic: 2.84 us -> none  [the longest x1 1.77 us: local(): (resid + moe + jax.nn.sigmoid(dense_mix) * dense).astype(jnp.bfloat16)]
  transfers between devices with their start and end apart: 6 -> 0, of which waited for: 6 -> 0; matrix products, arithmetic and copies ran while one was open for 12% -> 0% of each run, Pallas kernels for 0% -> 0%
where the time goes in v1:
time: 82.7 us; the launch traced here: 82.3 us
  Pallas kernels  49.1 us (59%)
  matrix products  16.9 us (20%)
  other arithmetic  12.1 us (15%)
  local copies, waits for them, and re-layouts  3.33 us (4%)
  between operations  0.85 us (1%)
    pallas_call x1, Pallas kernels, channel_mixers(): pl.pallas_call(functools.partial(channel_kernel, E, T), out_shape=jax.Sha...  49.1 us
    add x1, other arithmetic, local(): keep[..., None] * state + write[..., None] * values[:, :, None, :]  10.7 us
    dot_general x1, matrix products, local(): jnp.einsum('thk,thkv->thv', query, new_state, precision=lax.Precision.HIG...  9.38 us
    dot_general x1, matrix products, local(): block_term = jnp.dot(headout, w_out, preferred_element_type=jnp.float32)  2.55 us
    unnamed x21, local copies, waits for them, and re-layouts  2.54 us
    dot_general x1, matrix products, local(): zf = jnp.dot(normed, w_forget, preferred_element_type=jnp.float32)  2.35 us
    dot_general x1, matrix products, local(): zi = jnp.dot(normed, w_input, preferred_element_type=jnp.float32)  2.1 us

profile of v1, /device:TPU:0, one launch (start us, length us, event | category | flops | bytes accessed | tf_op | source)
XLA Modules:
  0.0 82.3 jit_solution(8950440747658544640)
XLA Ops:
  0.6 0.0 copy-start
  0.6 0.0 copy-start.1
  0.7 0.0 copy-start.8
  0.7 1.2 %fusion.1 = f32[32]{0:T(128)S(1)} fusion(bf16[32,2048]{1,0:T(8,128)(2,1)} %param.20), kind=kLoop, calls=%fused_computation.5 | loop fusion | flops 196576 | bytes 131200 | tf_op jit(solution)/shard_map/reduce_sum | solution.py:14
  1.9 0.7 log.3
  2.6 2.3 %fusion.11 = (f32[32,512]{1,0:T(8,128)S(1)}, f32[32,512]{1,0:T(8,128)S(1)}) fusion(f32[512]{0:T(512)S(1)} %log.3, bf16[2048,512]{1,0:T(8,128)(2,1)} %param.24, bf16[32,2048]{1,0:T(8,128)(2,1)} %param.20, f32[2048]{0:T(1024)} %param.22, f32[32]{0:T(128)S(1)} %add_rsqrt_fusion.1), kind=kOutput, calls=%fused_computation.24 | convolution fusion | flops 67780608 | bytes 2369664 | tf_op jit(solution)/shard_map/dot_general | solution.py:423
  5.0 0.0 copy-done.1
  5.0 0.0 copy-done.8
  5.0 2.1 %fusion.14 = f32[32,512]{1,0:T(8,128)S(1)} fusion(bf16[2048,512]{1,0:T(8,128)(2,1)} %param.25, bf16[32,2048]{1,0:T(8,128)(2,1)S(1)} %copy-done.1, f32[2048]{0:T(1024)S(1)} %copy-done.8, f32[32]{0:T(128)S(1)} %add_rsqrt_fusion.1), kind=kOutput, calls=%fused_computation.26 | convolution fusion | flops 67371008 | bytes 2302080 | tf_op jit(solution)/shard_map/dot_general | solution.py:424
  7.1 0.0 copy-start.7
  7.1 10.7 %multiply_add_fusion = f32[32,4,128,128]{3,2,1,0:T(8,128)} fusion(f32[32,4,128,128]{3,2,1,0:T(8,128)} %param.21, f32[32,4,128]{2,1,0:T(4,128)S(1)} %mul.80, f32[32,4,128]{2,1,0:T(4,128)S(1)} %neg.49, f32[32,4,128]{2,1,0:T(4,128)S(1)} %exp.33), kind=kLoop, calls=%fused_computation | loop fusion | flops 6291456 | bytes 16973824 | tf_op jit(solution)/shard_map/add | solution.py:432
  17.8 0.0 copy-done.7
  17.8 0.5 divide_multiply_fusion
  18.4 0.0 copy-start.9
  18.4 9.4 %fusion.26 = f32[32,4,1,128]{3,2,1,0:T(1,128)S(1)} fusion(f32[32,4,128,1]{2,3,1,0:T(1,128)S(1)} %bitcast.43, f32[32,4,128,128]{3,2,1,0:T(8,128)} %multiply_add_fusion), kind=kOutput, calls=%fused_computation.29 | convolution fusion | flops 25165824 | bytes 8519680 | tf_op jit(solution)/shard_map/thk,thkv->thv/dot_general | solution.py:433
  27.8 0.1 multiply_reduce_fusion
  27.9 0.0 copy-done.9
  27.9 0.1 multiply_multiply_fusion
  28.0 0.0 copy-done
  28.0 0.0 copy-start.3
  28.0 0.0 copy-start.4
  28.0 0.0 copy-start.5
  28.1 0.0 copy-start.6
  28.1 2.6 %fusion.bt_ref = bf16[4,8,2048]{2,1,0:T(8,128)(2,1)S(1)} fusion(bf16[512,2048]{1,0:T(8,128)(2,1)S(1)} %copy-done, f32[4,8,4,128]{3,2,1,0:T(4,128)S(1)} %bitcast.42, bf16[2048,512]{1,0:T(8,128)(2,1)} %param.26, bf16[32,2048]{1,0:T(8,128)(2,1)S(1)} %copy-done.1, f32[2048]{0:T(1024)S(1)} %copy-done.8, f32[32]{0:T(128)S(1)} %add_rsqrt_fusion.1), kind=kOutput, calls=%fused_computation.2 | convolution fusion | flops 134643712 | bytes 4530304 | tf_op jit(solution)/shard_map/dot_general | solution.py:436
  30.6 0.0 copy-done.3
  30.6 0.0 copy-done.4
  30.7 0.0 copy-done.5
  30.7 0.0 copy-done.6
  30.7 0.0 copy-start.2
  30.7 1.8 %copy-done.2 = bf16[2048,704]{0,1:T(8,128)(2,1)S(1)} copy-done((bf16[2048,704]{0,1:T(8,128)(2,1)S(1)}, bf16[2048,704]{0,1:T(8,128)(2,1)}, u32[]{:S(2)}) %copy-start.2) | copy-done | bytes 2883608
  32.5 49.1 %channel_mixers.1 = bf16[4,8,2048]{2,1,0:T(8,128)(2,1)S(1)} custom-call(bf16[4,8,2048]{2,1,0:T(8,128)(2,1)S(1)} %bitcast.29, bf16[4,8,2048]{2,1,0:T(8,128)(2,1)S(1)} %fusion.bt_ref, f32[1,2048]{1,0:T(1,128)S(1)} %bitcast.32, f32[1,2048]{1,0:T(1,128)S(1)} %bitcast.33, s32[2,32]{1,0:T(2,128)S(1)} %bitcast.34, f32[2,32]{1,0:T(2,128)S(1)} %bitcast.35, ...), custom_call_target="tpu_custom_call" | custom-call | tf_op jit(solution)/shard_map/channel_mixers/pallas_call | solution.py:327
  81.6 0.7 copy.28
  (6 shorter events, 0.1 us)
Async XLA Ops:
  0.6 27.4 %copy-start = (bf16[512,2048]{1,0:T(8,128)(2,1)S(1)}, bf16[512,2048]{1,0:T(8,128)(2,1)}, u32[]{:S(2)}) copy-start(bf16[512,2048]{1,0:T(8,128)(2,1)} %param.29) | copy-start | bytes 6291460
  0.6 4.3 %copy-start.1 = (bf16[32,2048]{1,0:T(8,128)(2,1)S(1)}, bf16[32,2048]{1,0:T(8,128)(2,1)}, u32[]{:S(2)}) copy-start(bf16[32,2048]{1,0:T(8,128)(2,1)} %param.20) | copy-start | bytes 393220
  0.7 4.3 %copy-start.8 = (f32[2048]{0:T(1024)S(1)}, f32[2048]{0:T(1024)}, u32[]{:S(2)}) copy-start(f32[2048]{0:T(1024)} %param.22) | copy-start | bytes 24580
  7.1 10.7 %copy-start.7 = (bf16[2048,512]{1,0:T(8,128)(2,1)S(1)}, bf16[2048,512]{1,0:T(8,128)(2,1)}, u32[]{:S(2)}) copy-start(bf16[2048,512]{1,0:T(8,128)(2,1)} %param.23) | copy-start | bytes 6291460
  18.4 9.5 %copy-start.9 = (f32[128]{0:T(128)S(1)}, f32[128]{0:T(128)}, u32[]{:S(2)}) copy-start(f32[128]{0:T(128)} %param.28) | copy-start | bytes 1540
  28.0 2.6 %copy-start.3 = (f32[2048]{0:T(1024)S(1)}, f32[2048]{0:T(1024)}, u32[]{:S(2)}) copy-start(f32[2048]{0:T(1024)} %param.30) | copy-start | bytes 24580
  28.0 2.6 %copy-start.4 = (f32[2048]{0:T(1024)S(1)}, f32[2048]{0:T(1024)}, u32[]{:S(2)}) copy-start(f32[2048]{0:T(1024)} %param.39) | copy-start | bytes 24580
  28.0 2.6 %copy-start.5 = (s32[32,2]{0,1:T(2,128)S(1)}, s32[32,2]{0,1:T(2,128)}, u32[]{:S(2)}) copy-start(s32[32,2]{0,1:T(2,128)} %param.31) | copy-start | bytes 772
  28.1 2.6 %copy-start.6 = (f32[32,2]{0,1:T(2,128)S(1)}, f32[32,2]{0,1:T(2,128)}, u32[]{:S(2)}) copy-start(f32[32,2]{0,1:T(2,128)} %param.32) | copy-start | bytes 772
  30.7 1.8 %copy-start.2 = (bf16[2048,704]{0,1:T(8,128)(2,1)S(1)}, bf16[2048,704]{0,1:T(8,128)(2,1)}, u32[]{:S(2)}) copy-start(bf16[2048,704]{0,1:T(8,128)(2,1)} %param.36) | copy-start | bytes 8650756

commit v2 on v1

--- a/solution.py
+++ b/solution.py
@@ -371,7 +371,7 @@
             dma((T,)),
         ],
         compiler_params=pltpu.CompilerParams(
-            collective_id=0, has_side_effects=True, vmem_limit_bytes=50 * 1024 * 1024
+            collective_id=0, has_side_effects=True, vmem_limit_bytes=62 * 1024 * 1024
         ),
         name="channel_mixers",
     )(
@@ -389,6 +389,159 @@
         dd,
     )
     return out.reshape(seqs, width)
+
+
+def mixer_kernel(
+    chunk,
+    tok_ref,
+    gain_ref,
+    floor_ref,
+    hgain_ref,
+    wq_hbm,
+    wf_hbm,
+    wi_hbm,
+    wo_hbm,
+    w_hbm,
+    state_hbm,
+    new_hbm,
+    term_ref,
+    wq,
+    wf,
+    wi,
+    wo,
+    w,
+    st,
+    keep_t,
+    query_t,
+    vals,
+    outgate,
+    read_ref,
+    w_sem,
+    in_sem,
+    out_sem,
+):
+    seqs, heads, key_size, value_size = st.shape
+    chunks = seqs // chunk
+
+    def load_state(n):
+        at = pl.ds(n * chunk, chunk)
+        return pltpu.make_async_copy(state_hbm.at[at], st.at[at], in_sem.at[n])
+
+    def store_state(n):
+        at = pl.ds(n * chunk, chunk)
+        return pltpu.make_async_copy(st.at[at], new_hbm.at[at], out_sem.at[n])
+
+    load_f = pltpu.make_async_copy(wf_hbm, wf, w_sem.at[0])
+    load_q = pltpu.make_async_copy(wq_hbm, wq, w_sem.at[1])
+    load_i = pltpu.make_async_copy(wi_hbm, wi, w_sem.at[2])
+    load_o = pltpu.make_async_copy(wo_hbm, wo, w_sem.at[3])
+    load_w = pltpu.make_async_copy(w_hbm, w, w_sem.at[4])
+    load_f.start()
+    load_q.start()
+    load_i.start()
+    for n in range(chunks):
+        load_state(n).start()
+    load_o.start()
+    load_w.start()
+
+    normed = rms_norm(tok_ref[...].astype(jnp.float32), gain_ref[...]).astype(jnp.bfloat16)
+
+    def turned(value, ref):
+        for h in range(heads):
+            column = value[:, h * key_size : (h + 1) * key_size].T
+            for n in range(chunks):
+                ref[n, h] = column[:, n * chunk : (n + 1) * chunk]
+
+    load_f.wait()
+    zf = jnp.dot(normed, wf[...], preferred_element_type=jnp.float32)
+    floor = floor_ref[...]
+    turned(floor + (1.0 - floor) * jax.nn.sigmoid(zf), keep_t)
+    load_q.wait()
+    zq = jnp.dot(normed, wq[...], preferred_element_type=jnp.float32)
+    turned(jax.nn.silu(zq), query_t)
+    load_i.wait()
+    vals[...] = jnp.dot(normed, wi[...], preferred_element_type=jnp.float32)
+
+    @pl.loop(0, chunks)
+    def _(n):
+        load_state(n).wait()
+        first = pl.multiple_of(n * chunk, chunk)
+        for h in range(heads):
+            lanes = slice(h * value_size, (h + 1) * value_size)
+            value = vals[pl.ds(first, chunk), lanes]
+            keep = keep_t[n, h]
+            query = query_t[n, h]
+            reads = []
+            for i in range(chunk):
+                row = value[i : i + 1]
+                new = row + keep[:, i : i + 1] * (st[first + i, h] - row)
+                st[first + i, h] = new
+                reads.append(jnp.sum(query[:, i : i + 1] * new, axis=0, keepdims=True))
+            read_ref[pl.ds(first, chunk), lanes] = jnp.concatenate(reads, axis=0)
+        store_state(n).start()
+
+    load_o.wait()
+    zg = jnp.dot(normed, wo[...], preferred_element_type=jnp.float32)
+    outgate[...] = jax.nn.silu(zg)
+    parts = []
+    for h in range(heads):
+        lanes = slice(h * value_size, (h + 1) * value_size)
+        parts.append(rms_norm(read_ref[:, lanes], hgain_ref[...]) * outgate[:, lanes])
+    headout = jnp.concatenate(parts, axis=1).astype(jnp.bfloat16)
+    load_w.wait()
+    term_ref[...] = jnp.dot(headout, w[...], preferred_element_type=jnp.float32).astype(jnp.bfloat16)
+    for n in range(chunks):
+        store_state(n).wait()
+
+
+def mixer(tokens, state, norm_gain, weights, forget_floor, head_gain, w_out):
+    seqs, width = tokens.shape
+    _, heads, key_size, value_size = state.shape
+    chunk = 8
+    chunks = seqs // chunk
+    wq, wf, wi, wo = weights
+    f32, bf = jnp.float32, jnp.bfloat16
+    vmem, dma = pltpu.VMEM, pltpu.SemaphoreType.DMA
+    vm = pl.BlockSpec(memory_space=pltpu.VMEM)
+    hbm = pl.BlockSpec(memory_space=pl.ANY)
+    return pl.pallas_call(
+        functools.partial(mixer_kernel, chunk),
+        out_shape=(
+            jax.ShapeDtypeStruct(state.shape, f32),
+            jax.ShapeDtypeStruct((seqs, width), bf),
+        ),
+        in_specs=[vm] * 4 + [hbm] * 6,
+        out_specs=(hbm, vm),
+        scratch_shapes=[
+            vmem(wq.shape, bf),
+            vmem(wf.shape, bf),
+            vmem(wi.shape, bf),
+            vmem(wo.shape, bf),
+            vmem(w_out.shape, bf),
+            vmem(state.shape, f32),
+            vmem((chunks, heads, key_size, chunk), f32),
+            vmem((chunks, heads, key_size, chunk), f32),
+            vmem((seqs, heads * value_size), f32),
+            vmem((seqs, heads * value_size), f32),
+            vmem((seqs, heads * value_size), f32),
+            dma((5,)),
+            dma((chunks,)),
+            dma((chunks,)),
+        ],
+        compiler_params=pltpu.CompilerParams(vmem_limit_bytes=60 * 1024 * 1024),
+        name="mixer",
+    )(
+        tokens,
+        norm_gain.reshape(1, width),
+        forget_floor.reshape(1, heads * key_size),
+        head_gain.reshape(1, value_size),
+        wq,
+        wf,
+        wi,
+        wo,
+        w_out,
+        state,
+    )
 
 
 def local(
@@ -414,31 +567,21 @@
     dense_mix,
 ):
     seqs, width = tokens.shape
-    local_heads = state.shape[1]
-    key_size = state.shape[2]
-    value_size = state.shape[3]
     resid_in = tokens.astype(jnp.float32)
-    normed = rms_norm(resid_in, norm_gain).astype(jnp.bfloat16)
-    zq = jnp.dot(normed, w_query, preferred_element_type=jnp.float32)
-    zf = jnp.dot(normed, w_forget, preferred_element_type=jnp.float32)
-    zi = jnp.dot(normed, w_input, preferred_element_type=jnp.float32)
-    zg = jnp.dot(normed, w_outgate, preferred_element_type=jnp.float32)
-    logf = jnp.logaddexp(jax.nn.log_sigmoid(zf), jnp.log(forget_floor) + jax.nn.log_sigmoid(-zf))
-    logf = logf.reshape(seqs, local_heads, key_size)
-    query = jax.nn.silu(zq).reshape(seqs, local_heads, key_size)
-    keep = jnp.exp(logf)
-    write = -jnp.expm1(logf)
-    values = zi.reshape(seqs, local_heads, value_size)
-    new_state = keep[..., None] * state + write[..., None] * values[:, :, None, :]
-    read = jnp.einsum("thk,thkv->thv", query, new_state, precision=lax.Precision.HIGHEST)
-    read = rms_norm(read, head_gain).reshape(seqs, local_heads * value_size)
-    headout = (read * jax.nn.silu(zg)).astype(jnp.bfloat16)
-    block_term = jnp.dot(headout, w_out, preferred_element_type=jnp.float32)
+    new_state, block_term = mixer(
+        tokens,
+        state,
+        norm_gain,
+        (w_query, w_forget, w_input, w_outgate),
+        forget_floor,
+        head_gain,
+        w_out,
+    )
     ways = lax.axis_size("tp")
     if ways % 2 == 0 and seqs % (8 * ways) == 0 and dense_gate.shape[1] % (16 * ways) == 0:
         mixed = channel_mixers(
             tokens,
-            block_term.astype(jnp.bfloat16),
+            block_term,
             ffn_gain,
             dense_mix,
             routes,
@@ -447,8 +590,7 @@
             (dense_gate.T, dense_up.T, dense_down),
         )
         return (mixed, new_state)
-    block_term = block_term.astype(jnp.bfloat16).astype(jnp.float32)
-    mixout = lax.psum(block_term.astype(jnp.bfloat16), "tp").astype(jnp.float32)
+    mixout = lax.psum(block_term, "tp").astype(jnp.float32)
     resid = resid_in + mixout
     ffn_in = rms_norm(resid, ffn_gain).astype(jnp.bfloat16)
     piece = lax.all_gather(ffn_in, "ep", axis=0, tiled=True)

time: 82.7 us -> 64.9 us (0.78)
  matrix products: 16.9 us -> 0 us
  Pallas kernels: 49.1 us -> 62.5 us
  other arithmetic: 12.1 us -> 0 us
  local copies, waits for them, and re-layouts: 3.33 us -> 1.57 us
    dot_general x5 -> x0, matrix products: 16.9 us -> none  [the longest x1 9.38 us: local(): jnp.einsum('thk,thkv->thv', query, new_state, precision=lax.Precision.HIG...]
    pallas_call x0 -> x1, Pallas kernels: none -> 11.8 us  [mixer(): pl.pallas_call(functools.partial(mixer_kernel, chunk), out_shape=(jax.Sha...]
    add x1 -> x0, other arithmetic: 10.7 us -> none  [local(): keep[..., None] * state + write[..., None] * values[:, :, None, :]]
    pallas_call x1, Pallas kernels: 49.1 us -> 50.8 us  [channel_mixers(): pl.pallas_call(functools.partial(channel_kernel, E, T), out_shape=jax.Sha...]
    reduce_sum x2 -> x0, other arithmetic: 1.3 us -> none  [rms_norm(): jnp.mean(value * value, axis=-1, keepdims=True) + EPS]
    unnamed x21 -> x1, local copies, waits for them, and re-layouts: 2.54 us -> 1.57 us
where the time goes in v2:
time: 64.9 us; the launch traced here: 64.7 us
  Pallas kernels  62.5 us (96%)
  local copies, waits for them, and re-layouts  1.57 us (2%)
  between operations  0.65 us (1%)
    pallas_call x1, Pallas kernels, channel_mixers(): pl.pallas_call(functools.partial(channel_kernel, E, T), out_shape=jax.Sha...  50.8 us
    pallas_call x1, Pallas kernels, mixer(): pl.pallas_call(functools.partial(mixer_kernel, chunk), out_shape=(jax.Sha...  11.8 us
    unnamed x1, local copies, waits for them, and re-layouts  1.57 us

profile of v2, /device:TPU:0, one launch (start us, length us, event | category | flops | bytes accessed | tf_op | source)
XLA Modules:
  0.0 64.7 jit_solution(2938601343850724914)
XLA Ops:
  0.6 11.8 %mixer.1 = (f32[32,4,128,128]{3,2,1,0:T(8,128)}, bf16[32,2048]{1,0:T(8,128)(2,1)}) custom-call(bf16[32,2048]{1,0:T(8,128)(2,1)} %tok_ref.1, f32[1,2048]{1,0:T(1,128)} %bitcast.23, f32[1,512]{1,0:T(1,128)} %bitcast.26, f32[1,128]{1,0:T(1,128)} %bitcast.29, bf16[2048,512]{1,0:T(8,128)(2,1)} %wq_hbm.1, bf16[2048,512]{1,0:T(8,128)(2,1)} %wf_hbm.1, ...), custom_call_target="tpu_custom_call" | custom-call | tf_op jit(solution)/shard_map/mixer/pallas_call | solution.py:507
  12.4 50.8 %channel_mixers.1 = bf16[4,8,2048]{2,1,0:T(8,128)(2,1)} custom-call(bf16[4,8,2048]{2,1,0:T(8,128)(2,1)} %bitcast.20, bf16[4,8,2048]{2,1,0:T(8,128)(2,1)} %bitcast.22, f32[1,2048]{1,0:T(1,128)} %bitcast.24, f32[1,2048]{1,0:T(1,128)} %bitcast.25, s32[2,32]{1,0:T(2,128)} %bitcast.27, f32[2,32]{1,0:T(2,128)} %bitcast.28, bf16[2048,1408]{1,0:T(8,128)(2,1)} %bitcast.15, ...), custom_call_target="tpu_custom_call" | custom-call | tf_op jit(solution)/shard_map/channel_mixers/pallas_call | solution.py:327
  63.2 1.6 %copy.23 = bf16[32,2048]{1,0:T(8,128)(2,1)} copy(bf16[32,2048]{1,0:T(8,128)(2,1)} %bitcast.21) | data formatting | bytes 262144
